TPU v7x, 32 devices: a whole 2x2x4 slice. The times are simulated.
32 devices in a mesh: sp: 4 (over z), tp: 4 (over y, x), dp: 2 (over core).
Axes of the slice: x: 2, y: 2, z: 4, core: 2. Of those that a mesh axis runs over, the one named last changes fastest.
Arguments:
- latent: bfloat16 [4, 4096, 2048], P('dp', 'sp'), may hold values from -6 to 6
- context: bfloat16 [4, 1024, 2048], P('dp', 'sp'), may hold values from -6 to 6
- condition: bfloat16 [4, 2048], P('dp', 'sp'), may hold values from -6 to 6
- ctx_cond: bfloat16 [2048], P('sp'), may hold values from -6 to 6
- norm_gain: float32 [2048], replicated, may hold values from 0.1 to 1.9
- w_shift: bfloat16 [2048, 2048], P('sp', 'tp'), may hold values from -0.125 to 0.125
- w_scale: bfloat16 [2048, 2048], P('sp', 'tp'), may hold values from -0.125 to 0.125
- w_gate: bfloat16 [2048, 2048], P('sp', 'tp'), may hold values from -0.125 to 0.125
- w_query: bfloat16 [2048, 1024], P(None, 'tp'), may hold values from -0.125 to 0.125
- w_key: bfloat16 [2048, 256], P(None, 'tp'), may hold values from -0.125 to 0.125
- w_value: bfloat16 [2048, 256], P(None, 'tp'), may hold values from -0.125 to 0.125
- w_out: bfloat16 [1024, 2048], P('tp'), may hold values from -4 to 4
- sink_logit: float32 [16], P('tp'), may hold values from 4 to 7
- ctx_lift: float32 [16], P('tp'), may hold values from -4 to 220
Outputs:
- mixed: bfloat16 [4, 4096, 2048], P('dp', ('sp', 'tp'))
All inputs are finite; a program needn't handle non-finite values.
Results may differ from a plain program's by a relative error of at most 0.012.
Values may be sent and summed in bfloat16 or wider, within the bound.
A program may use at most 128 MiB of HBM per device.

v0:
```python
import jax
import jax.numpy as jnp
from jax import lax
from jax.sharding import PartitionSpec as P

HEAD = 64
WINDOW = 128
GRID_COLS = 64
epsilon = 1e-06
rope_base = 10000.0
masked_value = -1e30


def with_halo(cells, sides, width):
    for axis, dim in sides:
        count = lax.axis_size(axis)
        ends = count - 1
        head = lax.slice_in_dim(cells, 0, width, axis=dim)
        tail = lax.slice_in_dim(cells, cells.shape[dim] - width, cells.shape[dim], axis=dim)
        cells = jnp.concatenate(
            [
                lax.ppermute(tail, axis, [(i, (i + 1) % count) for i in range(ends)]),
                cells,
                lax.ppermute(head, axis, [((i + 1) % count, i) for i in range(ends)]),
            ],
            axis=dim,
        )
    return cells


def modulated(inputs, norm_gain, shift_vec, scale_vec):
    widened = inputs.astype(jnp.float32)
    inverse = lax.rsqrt(jnp.mean(widened * widened, axis=-1, keepdims=True) + epsilon)
    return (widened * inverse * norm_gain * (1.0 + scale_vec) + shift_vec).astype(jnp.bfloat16)


def rotate_half(half_part, angles):
    first_half, second = jnp.split(half_part, 2, axis=-1)
    cosine = jnp.cos(angles)[:, None, :]
    sine_part = jnp.sin(angles)[:, None, :]
    return jnp.concatenate(
        [first_half * cosine - second * sine_part, first_half * sine_part + second * cosine],
        axis=-1,
    )


def rotate(inputs, positions):
    quarter = inputs.shape[-1] // 4
    frequency = rope_base ** (-jnp.arange(quarter, dtype=jnp.float32) / quarter)
    row_angle = (positions // GRID_COLS).astype(jnp.float32)[:, None] * frequency
    col_angle = (positions % GRID_COLS).astype(jnp.float32)[:, None] * frequency
    half_size = 2 * quarter
    return jnp.concatenate(
        [
            rotate_half(inputs[..., :half_size], row_angle),
            rotate_half(inputs[..., half_size:], col_angle),
        ],
        axis=-1,
    )


def shards(
    latent,
    context,
    condition,
    ctx_cond,
    norm_gain,
    w_shift,
    w_scale,
    w_gate,
    w_query,
    w_key,
    w_value,
    w_out,
    sink_logit,
    ctx_lift,
):
    samples, tokens, model_width = latent.shape
    head_size = HEAD
    sp_count = lax.axis_size("sp")
    cond_rows = jnp.concatenate([condition, ctx_cond[None, :]], axis=0)
    active = jax.nn.silu(cond_rows.astype(jnp.float32)).astype(jnp.bfloat16)
    shift_part, scale_part, gate_part = lax.psum(
        (
            jnp.dot(active, w_shift, preferred_element_type=jnp.float32),
            jnp.dot(active, w_scale, preferred_element_type=jnp.float32),
            jnp.dot(active, w_gate, preferred_element_type=jnp.float32),
        ),
        "sp",
    )
    shift_vec, scale_vec, gate_vec = (
        lax.all_gather(shift_part, "tp", axis=1, tiled=True),
        lax.all_gather(scale_part, "tp", axis=1, tiled=True),
        lax.all_gather(gate_part, "tp", axis=1, tiled=True),
    )
    hidden = modulated(
        latent, norm_gain, shift_vec[:samples, None, :], scale_vec[:samples, None, :]
    )
    offset_row = lax.axis_index("sp") * tokens
    positions = offset_row + jnp.arange(tokens, dtype=jnp.int32)
    query_heads = w_query.shape[1] // head_size
    key_heads = w_key.shape[1] // head_size
    group_size = query_heads // key_heads
    keyed = key_heads * head_size
    queries = rotate(
        jnp.einsum("snd,dc->snc", hidden, w_query, preferred_element_type=jnp.float32).reshape(
            samples, tokens, query_heads, head_size
        ),
        positions,
    ).astype(jnp.bfloat16)
    key_rows = rotate(
        jnp.einsum("snd,dc->snc", hidden, w_key, preferred_element_type=jnp.float32).reshape(
            samples, tokens, key_heads, head_size
        ),
        positions,
    ).astype(jnp.bfloat16)
    values = jnp.einsum("snd,dc->snc", hidden, w_value, preferred_element_type=jnp.float32).astype(
        jnp.bfloat16
    )
    local_pairs = jnp.concatenate([key_rows.reshape(samples, tokens, keyed), values], axis=-1)
    extended = with_halo(local_pairs, (("sp", 1),), WINDOW)
    ctx_hidden = modulated(context, norm_gain, shift_vec[samples], scale_vec[samples])
    ctx_keys = jnp.einsum(
        "snd,dc->snc", ctx_hidden, w_key, preferred_element_type=jnp.float32
    ).astype(jnp.bfloat16)
    ctx_values = jnp.einsum(
        "snd,dc->snc", ctx_hidden, w_value, preferred_element_type=jnp.float32
    ).astype(jnp.bfloat16)
    context_pairs = lax.all_gather(
        jnp.concatenate([ctx_keys, ctx_values], axis=-1), "sp", axis=1, tiled=True
    )
    block_rows = min(512, tokens)
    blocks = tokens // block_rows
    span_rows = block_rows + 2 * WINDOW
    latent_len = tokens * sp_count
    lift_rows = ctx_lift.reshape(key_heads, group_size, 1, 1)
    sink_rows = sink_logit.reshape(key_heads, group_size, 1, 1)
    factor = head_size ** (-0.5)

    def attend(step_id):
        sample = step_id // blocks
        row_start = step_id % blocks * block_rows
        q_rows = lax.dynamic_slice_in_dim(
            lax.dynamic_index_in_dim(queries, sample, 0, keepdims=False), row_start, block_rows, 0
        )
        q_rows = q_rows.reshape(block_rows, key_heads, group_size, head_size)
        pair_rows = lax.dynamic_slice_in_dim(
            lax.dynamic_index_in_dim(extended, sample, 0, keepdims=False), row_start, span_rows, 0
        )
        near_keys = pair_rows[:, :keyed].reshape(span_rows, key_heads, head_size)
        near_values = pair_rows[:, keyed:].reshape(span_rows, key_heads, head_size)
        ctx_rows = lax.dynamic_index_in_dim(context_pairs, sample, 0, keepdims=False)
        far_keys = ctx_rows[:, :keyed].reshape(-1, key_heads, head_size)
        far_values = ctx_rows[:, keyed:].reshape(-1, key_heads, head_size)
        query_pos = offset_row + row_start + jnp.arange(block_rows, dtype=jnp.int32)
        key_pos = offset_row + row_start - WINDOW + jnp.arange(span_rows, dtype=jnp.int32)
        inside = (
            (key_pos[None, :] >= 0)
            & (key_pos[None, :] < latent_len)
            & (jnp.abs(query_pos[:, None] - key_pos[None, :]) <= WINDOW)
        )
        near_scores = (
            jnp.einsum("qgrd,kgd->grqk", q_rows, near_keys, preferred_element_type=jnp.float32)
            * factor
        )
        near_scores = jnp.where(inside[None, None], near_scores, masked_value)
        far_scores = (
            jnp.einsum("qgrd,kgd->grqk", q_rows, far_keys, preferred_element_type=jnp.float32)
            * factor
            + lift_rows
        )
        row_max = jnp.maximum(
            jnp.maximum(near_scores.max(-1, keepdims=True), far_scores.max(-1, keepdims=True)),
            sink_rows,
        )
        near_exp = jnp.exp(near_scores - row_max)
        far_exp = jnp.exp(far_scores - row_max)
        normaliser = (
            near_exp.sum(-1, keepdims=True)
            + far_exp.sum(-1, keepdims=True)
            + jnp.exp(sink_rows - row_max)
        )
        outcome = jnp.einsum(
            "grqk,kgd->qgrd",
            (near_exp / normaliser).astype(jnp.bfloat16),
            near_values,
            preferred_element_type=jnp.float32,
        )
        outcome = outcome + jnp.einsum(
            "grqk,kgd->qgrd",
            (far_exp / normaliser).astype(jnp.bfloat16),
            far_values,
            preferred_element_type=jnp.float32,
        )
        return outcome.astype(jnp.bfloat16).reshape(block_rows, query_heads * head_size)

    attended = lax.map(attend, jnp.arange(samples * blocks, dtype=jnp.int32)).reshape(
        samples, tokens, query_heads * head_size
    )
    by_rows = lax.all_to_all(attended, "tp", split_axis=1, concat_axis=2, tiled=True)
    projected = jnp.einsum(
        "snc,cd->snd",
        by_rows,
        lax.all_gather(w_out, "tp", axis=0, tiled=True),
        preferred_element_type=jnp.float32,
    )
    return (gate_vec[:samples, None, :] * projected).astype(jnp.bfloat16)


def solution(mesh):
    return jax.shard_map(
        shards,
        mesh=mesh,
        in_specs=(
            P("dp", "sp", None),
            P("dp", "sp", None),
            P("dp", "sp"),
            P("sp"),
            P(),
            P("sp", "tp"),
            P("sp", "tp"),
            P("sp", "tp"),
            P(None, "tp"),
            P(None, "tp"),
            P(None, "tp"),
            P("tp", None),
            P("tp"),
            P("tp"),
        ),
        out_specs=P("dp", ("sp", "tp"), None),
        check_vma=False,
    )
```

profile of v0, /device:TPU:0, one launch (start us, length us, event | category | flops | bytes accessed | tf_op | source)
XLA Modules:
  0.0 226.5 jit_solution(14336475768110559586)
XLA Ops:
  6.6 0.8 broadcast_in_dim.31
  7.3 1.2 fusion.70
  8.6 1.2 fusion.72
  9.8 1.2 fusion.74
  11.1 21.3 %all-reduce = (f32[3,512]{1,0:T(4,128)S(1)}, f32[3,512]{1,0:T(4,128)S(1)}, f32[3,512]{1,0:T(4,128)}) all-reduce(f32[3,512]{1,0:T(4,128)S(1)} %fusion.70, f32[3,512]{1,0:T(4,128)S(1)} %fusion.72, f32[3,512]{1,0:T(4,128)S(1)} %fusion.74), channel_id=1, replica_groups=mesh['sp'=4,'tp'=4,'dp'=2] {'sp'}, use_global_device_ids=true, to_apply=%region_3.4 | all-reduce | flops 4608 | bytes 36864 | tf_op jit(solution)/shard_map/psum | solution.py:83
  32.3 8.2 %all_gather.17 = f32[3,2048]{1,0:T(4,128)S(1)} all-gather(f32[3,512]{1,0:T(4,128)S(1)} %get-tuple-element.178), channel_id=1, replica_groups=mesh['sp'=4,'tp'=4,'dp'=2] {'tp'}, dimensions={1}, use_global_device_ids=true | all-gather | bytes 30720 | tf_op jit(solution)/shard_map/all_gather | solution.py:92
  40.5 8.2 %all_gather.16 = f32[3,2048]{1,0:T(4,128)S(1)} all-gather(f32[3,512]{1,0:T(4,128)S(1)} %get-tuple-element.179), channel_id=1, replica_groups=mesh['sp'=4,'tp'=4,'dp'=2] {'tp'}, dimensions={1}, use_global_device_ids=true | all-gather | bytes 30720 | tf_op jit(solution)/shard_map/all_gather | solution.py:93
  48.7 5.1 %fusion.26 = f32[2,1024]{1,0:T(2,128)S(1)} fusion(bf16[2,1024,2048]{2,1,0:T(8,128)(2,1)} %param.16), kind=kLoop, calls=%fused_computation.44 | loop fusion | flops 12580864 | bytes 8396800 | tf_op jit(solution)/shard_map/reduce_sum | solution.py:33
  53.8 0.5 multiply_cosine_fusion
  54.4 6.0 %convolution_bitcast_fusion = f32[2,1024,1,64]{1,3,0,2:T(8,128)S(1)} fusion(bf16[2,1024,2048]{2,1,0:T(8,128)(2,1)} %param.16, f32[2,2048]{1,0:T(2,128)S(1)} %slice.74, f32[2,2048]{1,0:T(2,128)S(1)} %slice_add_fusion, f32[2048]{0:T(1024)S(1)} %copy-done.6, f32[2,1024]{1,0:T(2,128)S(1)} %add_rsqrt_fusion, bf16[2048,64]{0,1:T(8,128)(2,1)S(1)} %copy-done.5), kind=kOutput, calls=%fused_computation.59 | convolution fusion | flops 562036736 | bytes 9224192 | tf_op jit(solution)/shard_map/snd,dc->snc/dot_general | solution.py:112
  60.5 6.9 %fusion.40 = bf16[2,1024,128]{1,2,0:T(8,128)(2,1)S(1)} fusion(bf16[2,1024,128]{1,2,0:T(8,128)(2,1)S(1)} %fusion.59, bf16[2,1024,2048]{2,1,0:T(8,128)(2,1)} %param.16, f32[2,2048]{1,0:T(2,128)S(1)} %slice.74, f32[2,2048]{1,0:T(2,128)S(1)} %slice_add_fusion, f32[2048]{0:T(1024)S(1)} %copy-done.6, f32[2,1024]{1,0:T(2,128)S(1)} %add_rsqrt_fusion, ...), kind=kOutput, calls=%fused_computation.61 | convolution fusion | flops 562167808 | bytes 8962048 | tf_op jit(solution)/shard_map/snd,dc->snc/dot_general | solution.py:117
  67.5 1.3 collective-permute-start
  68.8 1.5 collective-permute-start.1
  70.4 2.1 fusion.31
  72.4 2.6 %convolution_convert_fusion.1 = bf16[2,256,64]{1,2,0:T(8,128)(2,1)S(1)} fusion(bf16[2,256,2048]{2,1,0:T(8,128)(2,1)} %param.17, f32[2048]{0:T(1024)S(1)} %bitcast.202, f32[2048]{0:T(1024)S(1)} %bitcast.200, f32[2048]{0:T(1024)S(1)} %copy-done.6, f32[2,256]{1,0:T(2,128)S(1)} %add_rsqrt_fusion.1, bf16[2048,64]{0,1:T(8,128)(2,1)S(1)} %copy-done.4), kind=kOutput, calls=%fused_computation.62 | convolution fusion | flops 140541952 | bytes 2451456 | tf_op jit(solution)/shard_map/snd,dc->snc/dot_general | solution.py:126
  75.1 2.6 %convolution_convert_fusion.2 = bf16[2,256,64]{1,2,0:T(8,128)(2,1)S(1)} fusion(bf16[2,256,2048]{2,1,0:T(8,128)(2,1)} %param.17, f32[2048]{0:T(1024)S(1)} %bitcast.203, f32[2048]{0:T(1024)S(1)} %bitcast.201, f32[2048]{0:T(1024)S(1)} %copy-done.6, f32[2,256]{1,0:T(2,128)S(1)} %add_rsqrt_fusion.1, bf16[2048,64]{0,1:T(8,128)(2,1)S(1)} %copy-done.5), kind=kOutput, calls=%fused_computation.63 | convolution fusion | flops 140541952 | bytes 2451456 | tf_op jit(solution)/shard_map/snd,dc->snc/dot_general | solution.py:123
  77.7 6.7 %fusion.43 = f32[2,1024,256]{1,2,0:T(8,128)S(1)} fusion(bf16[2048,256]{1,0:T(8,128)(2,1)S(1)} %copy-done, bf16[2,1024,2048]{2,1,0:T(8,128)(2,1)} %param.16, f32[2,2048]{1,0:T(2,128)S(1)} %slice.74, f32[2,2048]{1,0:T(2,128)S(1)} %slice_add_fusion, f32[2048]{0:T(1024)S(1)} %copy-done.6, f32[2,1024]{1,0:T(2,128)S(1)} %add_rsqrt_fusion), kind=kOutput, calls=%fused_computation.65 | convolution fusion | flops 2172649472 | bytes 11583488 | tf_op jit(solution)/shard_map/snd,dc->snc/dot_general | solution.py:106
  84.8 15.8 %all_gather.18 = bf16[2,1024,128]{1,2,0:T(8,128)(2,1)S(1)} all-gather(bf16[2,256,128]{1,2,0:T(8,128)(2,1)S(1)} %pad_maximum_fusion.2), channel_id=1, replica_groups=mesh['sp'=4,'tp'=4,'dp'=2] {'sp'}, dimensions={1}, use_global_device_ids=true | all-gather | bytes 655360 | tf_op jit(solution)/shard_map/all_gather | solution.py:129
  100.7 0.9 pad_maximum_fusion.1
  101.6 0.6 iota.41
  102.2 91.8 %while.13 = (s32[]{:T(128)}, bf16[4,512,256]{2,1,0:T(8,128)(2,1)}, s32[4]{0:T(128)}, bf16[2,1280,128]{1,2,0:T(8,128)(2,1)}, s32[]{:T(128)}, /*index=5*/bf16[2,10...) while((s32[]{:T(128)}, bf16[4,512,256]{2,1,0:T(8,128)(2,1)}, ...), condition=%wide.region_10.11_spmd, body=%wide.region_5.10_spmd.sunk | while | flops 985405696 | bytes 75191968 | solution.py:197
  102.2 1.3 dynamic_slice.51
  105.8 4.6 %bitcast_reduce_fusion.2 = (f32[4,512]{1,0:T(4,128)S(1)}, f32[1024,512,4]{1,0,2:T(8,128)}) fusion(f32[4]{0:T(128)S(1)} %bitcast.194, bf16[2,1024,4,64]{1,3,2,0:T(8,128)(2,1)S(1)} %get-tuple-element.303, s32[]{:T(128)S(6)} %select_n.121, s32[]{:T(128)S(6)} %select_n.124, bf16[1024,128]{0,1:T(8,128)(2,1)S(1)} %dynamic-slice_bitcast_fusion.4), kind=kOutput, calls=%fused_computation.1.clone.1 | convolution fusion | flops 274724864 | bytes 8790536 | tf_op jit(solution)/shard_map/while/body/eval_jaxpr/qgrd,kgd->grqk/dot_general | solution.py:168
  110.4 0.5 fusion.91
  110.9 1.1 dynamic-slice_bitcast_fusion.5
  112.0 1.3 fusion.92
  113.4 5.2 %fusion.94 = f32[4,512]{1,0:T(4,128)S(1)} fusion(f32[1024,512,4]{1,0,2:T(8,128)} %get-tuple-element.260, f32[4,512]{1,0:T(4,128)S(1)} %maximum_maximum_fusion.2, f32[4]{0:T(128)S(1)} %bitcast.195), kind=kLoop, calls=%fused_computation.5.clone.1 | loop fusion | flops 8386560 | bytes 8405008 | tf_op jit(solution)/shard_map/while/body/eval_jaxpr/reduce_sum | solution.py:180
  118.7 1.4 fusion.93
  120.2 2.1 fusion.95
  122.3 2.0 fusion.96
  124.5 0.7 constant_dynamic-update-slice_fusion.2
  125.2 1.2 dynamic_slice.51
  128.8 4.6 %bitcast_reduce_fusion.2 = (f32[4,512]{1,0:T(4,128)S(1)}, f32[1024,512,4]{1,0,2:T(8,128)}) fusion(f32[4]{0:T(128)S(1)} %bitcast.194, bf16[2,1024,4,64]{1,3,2,0:T(8,128)(2,1)S(1)} %get-tuple-element.303, s32[]{:T(128)S(6)} %select_n.121, s32[]{:T(128)S(6)} %select_n.124, bf16[1024,128]{0,1:T(8,128)(2,1)S(1)} %dynamic-slice_bitcast_fusion.4), kind=kOutput, calls=%fused_computation.1.clone.1 | convolution fusion | flops 274724864 | bytes 8790536 | tf_op jit(solution)/shard_map/while/body/eval_jaxpr/qgrd,kgd->grqk/dot_general | solution.py:168
  133.3 0.5 fusion.91
  133.9 1.1 dynamic-slice_bitcast_fusion.5
  135.0 1.3 fusion.92
  136.4 5.2 %fusion.94 = f32[4,512]{1,0:T(4,128)S(1)} fusion(f32[1024,512,4]{1,0,2:T(8,128)} %get-tuple-element.260, f32[4,512]{1,0:T(4,128)S(1)} %maximum_maximum_fusion.2, f32[4]{0:T(128)S(1)} %bitcast.195), kind=kLoop, calls=%fused_computation.5.clone.1 | loop fusion | flops 8386560 | bytes 8405008 | tf_op jit(solution)/shard_map/while/body/eval_jaxpr/reduce_sum | solution.py:180
  141.6 1.4 fusion.93
  143.1 2.1 fusion.95
  145.2 2.0 fusion.96
  147.4 0.7 constant_dynamic-update-slice_fusion.2
  148.1 1.2 dynamic_slice.51
  151.7 4.6 %bitcast_reduce_fusion.2 = (f32[4,512]{1,0:T(4,128)S(1)}, f32[1024,512,4]{1,0,2:T(8,128)}) fusion(f32[4]{0:T(128)S(1)} %bitcast.194, bf16[2,1024,4,64]{1,3,2,0:T(8,128)(2,1)S(1)} %get-tuple-element.303, s32[]{:T(128)S(6)} %select_n.121, s32[]{:T(128)S(6)} %select_n.124, bf16[1024,128]{0,1:T(8,128)(2,1)S(1)} %dynamic-slice_bitcast_fusion.4), kind=kOutput, calls=%fused_computation.1.clone.1 | convolution fusion | flops 274724864 | bytes 8790536 | tf_op jit(solution)/shard_map/while/body/eval_jaxpr/qgrd,kgd->grqk/dot_general | solution.py:168
  156.3 0.5 fusion.91
  156.8 1.1 dynamic-slice_bitcast_fusion.5
  157.9 1.3 fusion.92
  159.3 5.2 %fusion.94 = f32[4,512]{1,0:T(4,128)S(1)} fusion(f32[1024,512,4]{1,0,2:T(8,128)} %get-tuple-element.260, f32[4,512]{1,0:T(4,128)S(1)} %maximum_maximum_fusion.2, f32[4]{0:T(128)S(1)} %bitcast.195), kind=kLoop, calls=%fused_computation.5.clone.1 | loop fusion | flops 8386560 | bytes 8405008 | tf_op jit(solution)/shard_map/while/body/eval_jaxpr/reduce_sum | solution.py:180
  164.6 1.4 fusion.93
  166.0 2.1 fusion.95
  168.2 2.0 fusion.96
  170.3 0.7 constant_dynamic-update-slice_fusion.2
  171.1 1.2 dynamic_slice.51
  174.6 4.6 %bitcast_reduce_fusion.2 = (f32[4,512]{1,0:T(4,128)S(1)}, f32[1024,512,4]{1,0,2:T(8,128)}) fusion(f32[4]{0:T(128)S(1)} %bitcast.194, bf16[2,1024,4,64]{1,3,2,0:T(8,128)(2,1)S(1)} %get-tuple-element.303, s32[]{:T(128)S(6)} %select_n.121, s32[]{:T(128)S(6)} %select_n.124, bf16[1024,128]{0,1:T(8,128)(2,1)S(1)} %dynamic-slice_bitcast_fusion.4), kind=kOutput, calls=%fused_computation.1.clone.1 | convolution fusion | flops 274724864 | bytes 8790536 | tf_op jit(solution)/shard_map/while/body/eval_jaxpr/qgrd,kgd->grqk/dot_general | solution.py:168
  179.8 1.1 dynamic-slice_bitcast_fusion.5
  180.8 1.3 fusion.92
  182.2 5.2 %fusion.94 = f32[4,512]{1,0:T(4,128)S(1)} fusion(f32[1024,512,4]{1,0,2:T(8,128)} %get-tuple-element.260, f32[4,512]{1,0:T(4,128)S(1)} %maximum_maximum_fusion.2, f32[4]{0:T(128)S(1)} %bitcast.195), kind=kLoop, calls=%fused_computation.5.clone.1 | loop fusion | flops 8386560 | bytes 8405008 | tf_op jit(solution)/shard_map/while/body/eval_jaxpr/reduce_sum | solution.py:180
  187.5 1.4 fusion.93
  189.0 2.1 fusion.95
  191.1 2.0 fusion.96
  193.3 0.7 constant_dynamic-update-slice_fusion.2
  194.0 3.3 %copy.27 = bf16[2,1024,256]{2,0,1:T(2,128)(2,1)} copy(bf16[2,1024,256]{2,1,0:T(8,128)(2,1)} %bitcast.191) | data formatting | bytes 2097152 | tf_op jit(solution)/shard_map/reshape | solution.py:197
  197.3 3.5 %all-to-all-start = ((bf16[2,1024,256]{2,0,1:T(2,128)(2,1)}), bf16[2,1024,256]{2,0,1:T(2,128)(2,1)S(1)}, u32[]{:S(2)}, u32[]{:S(2)}) async-start(bf16[2,1024,256]{2,0,1:T(2,128)(2,1)} %copy.27), calls=%async_computation | async-start | bytes 2097152 | tf_op jit(solution)/shard_map/all_to_all | solution.py:200
  200.8 12.7 %all_gather.15 = f32[3,2048]{1,0:T(4,128)S(1)} all-gather(f32[3,512]{1,0:T(4,128)S(1)} %copy-done.3), channel_id=1, replica_groups=mesh['sp'=4,'tp'=4,'dp'=2] {'tp'}, dimensions={1}, use_global_device_ids=true | all-gather | bytes 30720 | tf_op jit(solution)/shard_map/all_gather | solution.py:94
  213.8 5.8 %multiply_convert_fusion = bf16[2,256,2048]{2,1,0:T(8,128)(2,1)} fusion(bf16[2,256,1024]{2,1,0:T(8,128)(2,1)S(1)} %bitcast.192, bf16[1024,2048]{1,0:T(8,128)(2,1)} %all-gather.2.cloned.1.call-done, f32[2,2048]{1,0:T(2,128)S(1)} %slice.72), kind=kOutput, calls=%fused_computation.58 | convolution fusion | flops 2149580800 | bytes 7356416 | tf_op jit(solution)/shard_map/snc,cd->snd/dot_general | solution.py:201
  (89 shorter events, 2.9 us)
Async XLA Ops:
  6.5 71.2 %copy-start = (bf16[2048,256]{1,0:T(8,128)(2,1)S(1)}, bf16[2048,256]{1,0:T(8,128)(2,1)}, u32[]{:S(2)}) copy-start(bf16[2048,256]{1,0:T(8,128)(2,1)} %param.24) | copy-start | bytes 3145732
  6.5 47.8 %copy-start.6 = (f32[2048]{0:T(1024)S(1)}, f32[2048]{0:T(1024)}, u32[]{:S(2)}) copy-start(f32[2048]{0:T(1024)} %param.20) | copy-start | bytes 24580
  6.5 47.8 %copy-start.5 = (bf16[2048,64]{0,1:T(8,128)(2,1)S(1)}, bf16[2048,64]{0,1:T(8,128)(2,1)}, u32[]{:S(2)}) copy-start(bf16[2048,64]{0,1:T(8,128)(2,1)} %param.25) | copy-start | bytes 786436
  6.5 207.2 %all-gather.2.cloned.1.call-start = ((), (), s32[]{:S(2)}) async-start(), calls=%async_computation.1 | async-start | bytes 5242880 | tf_op jit(solution)/shard_map/all_gather | solution.py:204
  54.4 6.1 %copy-start.4 = (bf16[2048,64]{0,1:T(8,128)(2,1)S(1)}, bf16[2048,64]{0,1:T(8,128)(2,1)}, u32[]{:S(2)}) copy-start(bf16[2048,64]{0,1:T(8,128)(2,1)} %param.26) | copy-start | bytes 786436
  67.5 33.2 %collective-permute-start = (bf16[2,128,128]{1,2,0:T(8,128)(2,1)S(1)}, bf16[2,128,128]{1,2,0:T(8,128)(2,1)S(1)}, u32[]{:S(2)}, u32[]{:S(2)}) collective-permute-start(bf16[2,128,128]{1,2,0:T(8,128)(2,1)S(1)} %get-tuple-element.191), channel_id=1, source_target_pairs={{0,8},{8,16},{16,24},{1,9},{9,17},{17,25},{2,10},{10,18},{18,26},{... | collective-permute-start | bytes 196616 | tf_op jit(solution)/shard_map/ppermute | solution.py:22
  68.8 31.9 %collective-permute-start.1 = (bf16[2,128,128]{1,2,0:T(8,128)(2,1)S(1)}, bf16[2,128,128]{1,2,0:T(8,128)(2,1)S(1)}, u32[]{:S(2)}, u32[]{:S(2)}) collective-permute-start(bf16[2,128,128]{1,2,0:T(8,128)(2,1)S(1)} %get-tuple-element.192), channel_id=1, source_target_pairs={{8,0},{16,8},{24,16},{9,1},{17,9},{25,17},{10,2},{18,10},{26,18},{... | collective-permute-start | bytes 196616 | tf_op jit(solution)/shard_map/ppermute | solution.py:24
  84.4 17.8 %copy-start.1 = (f32[4]{0:T(128)S(1)}, f32[4]{0:T(128)}, u32[]{:S(2)}) copy-start(f32[4]{0:T(128)} %param.29) | copy-start | bytes 52
  84.4 17.8 %copy-start.2 = (f32[4]{0:T(128)S(1)}, f32[4]{0:T(128)}, u32[]{:S(2)}) copy-start(f32[4]{0:T(128)} %param.28) | copy-start | bytes 52
  102.2 98.6 %copy-start.3 = (f32[3,512]{1,0:T(4,128)S(1)}, f32[3,512]{1,0:T(4,128)}, u32[]{:S(2)}) copy-start(f32[3,512]{1,0:T(4,128)} %get-tuple-element.180) | copy-start | bytes 18436
  113.4 6.7 %slice-start = ((s8[8388608]{0:T(1024)(128)(4,1)}), s8[4194304]{0:T(1024)(128)(4,1)S(1)}, s32[]{:S(2)}) async-start(s8[8388608]{0:T(1024)(128)(4,1)} %bitcast.186), calls=%async_computation.2 | async-start | bytes 8388608 | tf_op jit(solution)/shard_map/while
  113.4 6.7 %slice-start.1 = ((s8[8388608]{0:T(1024)(128)(4,1)}), s8[4194304]{0:T(1024)(128)(4,1)S(1)}, s32[]{:S(2)}) async-start(s8[8388608]{0:T(1024)(128)(4,1)} %bitcast.186), calls=%async_computation.3 | async-start | bytes 8388608 | tf_op jit(solution)/shard_map/while
  136.4 6.7 %slice-start = ((s8[8388608]{0:T(1024)(128)(4,1)}), s8[4194304]{0:T(1024)(128)(4,1)S(1)}, s32[]{:S(2)}) async-start(s8[8388608]{0:T(1024)(128)(4,1)} %bitcast.186), calls=%async_computation.2 | async-start | bytes 8388608 | tf_op jit(solution)/shard_map/while
  136.4 6.7 %slice-start.1 = ((s8[8388608]{0:T(1024)(128)(4,1)}), s8[4194304]{0:T(1024)(128)(4,1)S(1)}, s32[]{:S(2)}) async-start(s8[8388608]{0:T(1024)(128)(4,1)} %bitcast.186), calls=%async_computation.3 | async-start | bytes 8388608 | tf_op jit(solution)/shard_map/while
  159.3 6.7 %slice-start = ((s8[8388608]{0:T(1024)(128)(4,1)}), s8[4194304]{0:T(1024)(128)(4,1)S(1)}, s32[]{:S(2)}) async-start(s8[8388608]{0:T(1024)(128)(4,1)} %bitcast.186), calls=%async_computation.2 | async-start | bytes 8388608 | tf_op jit(solution)/shard_map/while
  159.3 6.7 %slice-start.1 = ((s8[8388608]{0:T(1024)(128)(4,1)}), s8[4194304]{0:T(1024)(128)(4,1)S(1)}, s32[]{:S(2)}) async-start(s8[8388608]{0:T(1024)(128)(4,1)} %bitcast.186), calls=%async_computation.3 | async-start | bytes 8388608 | tf_op jit(solution)/shard_map/while
  182.2 6.7 %slice-start = ((s8[8388608]{0:T(1024)(128)(4,1)}), s8[4194304]{0:T(1024)(128)(4,1)S(1)}, s32[]{:S(2)}) async-start(s8[8388608]{0:T(1024)(128)(4,1)} %bitcast.186), calls=%async_computation.2 | async-start | bytes 8388608 | tf_op jit(solution)/shard_map/while
  182.2 6.7 %slice-start.1 = ((s8[8388608]{0:T(1024)(128)(4,1)}), s8[4194304]{0:T(1024)(128)(4,1)S(1)}, s32[]{:S(2)}) async-start(s8[8388608]{0:T(1024)(128)(4,1)} %bitcast.186), calls=%async_computation.3 | async-start | bytes 8388608 | tf_op jit(solution)/shard_map/while
  197.3 16.2 %all-to-all-start = ((bf16[2,1024,256]{2,0,1:T(2,128)(2,1)}), bf16[2,1024,256]{2,0,1:T(2,128)(2,1)S(1)}, u32[]{:S(2)}, u32[]{:S(2)}) async-start(bf16[2,1024,256]{2,0,1:T(2,128)(2,1)} %copy.27), calls=%async_computation | async-start | bytes 2097152 | tf_op jit(solution)/shard_map/all_to_all | solution.py:200
Sparse Core Ops, SparseCore 0:
  70.4 52.5 all-gather.1
where the time goes:
time: 227 us; the launch traced here: 226 us
  matrix products  74.6 us (33%)
  blocking collectives  66.1 us (29%)
  other arithmetic  38.5 us (17%)
  local copies, waits for them, and re-layouts  17.8 us (8%)
  between operations  13.7 us (6%)
  loops' own time  9.49 us (4%)
  starting transfers between devices  6.28 us (3%)
    psum x1, blocking collectives, shards(): lax.psum((jnp.dot(active, w_shift, preferred_element_type=jnp.float32), j...  21.3 us
    reduce_sum x4, other arithmetic, attend(): far_exp.sum(-1, keepdims=True)  21 us
    dot_general x4, matrix products, attend(): jnp.einsum('qgrd,kgd->grqk', q_rows, far_keys, preferred_element_type=jnp...  18.3 us
    all_gather x1, blocking collectives, shards(): lax.all_gather(jnp.concatenate([ctx_keys, ctx_values], axis=-1), 'sp', ax...  15.8 us
    all_gather x1, blocking collectives, shards(): lax.all_gather(gate_part, 'tp', axis=1, tiled=True)  12.7 us
    another operation x1, loops' own time, shards(): lax.map(attend, jnp.arange(samples * blocks, dtype=jnp.int32))  9.49 us
    dot_general x4, matrix products, attend(): jnp.einsum('grqk,kgd->qgrd', (far_exp / normaliser).astype(jnp.bfloat16),...  8.49 us
    all_gather x1, blocking collectives, shards(): lax.all_gather(shift_part, 'tp', axis=1, tiled=True)  8.18 us
  transfers between devices with their start and end apart: 4, of which 0 were waited for; matrix products, arithmetic and copies ran while one was open for 45% of the time, Pallas kernels for 0%

commit v1 on v0

--- a/solution.py
+++ b/solution.py
@@ -9,6 +9,23 @@
 epsilon = 1e-06
 rope_base = 10000.0
 masked_value = -1e30
+
+
+def in_order(blocks, dim):
+    lengths = list(blocks.shape[1:])
+    lengths[dim] *= blocks.shape[0]
+    return jnp.moveaxis(blocks, 0, dim).reshape(lengths)
+
+
+def collect(shard, axis, dim):
+    size = lax.axis_size(axis)
+    right = [(i, (i + 1) % size) for i in range(size)]
+    pieces = [shard]
+    while len(pieces) < size:
+        pieces.append(lax.ppermute(pieces[-1], axis, right))
+    index = lax.axis_index(axis)
+    pieces = jnp.stack(pieces)[(index - jnp.arange(size)) % size]
+    return in_order(pieces, dim)
 
 
 def with_halo(cells, sides, width):
@@ -126,9 +143,7 @@
     ctx_values = jnp.einsum(
         "snd,dc->snc", ctx_hidden, w_value, preferred_element_type=jnp.float32
     ).astype(jnp.bfloat16)
-    context_pairs = lax.all_gather(
-        jnp.concatenate([ctx_keys, ctx_values], axis=-1), "sp", axis=1, tiled=True
-    )
+    context_pairs = collect(jnp.concatenate([ctx_keys, ctx_values], axis=-1), "sp", 1)
     block_rows = min(512, tokens)
     blocks = tokens // block_rows
     span_rows = block_rows + 2 * WINDOW

time: 227 us -> 225 us (level)
  blocking collectives: 66.1 us -> 50.3 us
  waiting for transfers between devices: 0.05 us -> 11.4 us
  starting transfers between devices: 6.28 us -> 10.2 us
  matrix products: 74.6 us -> 71.2 us
    all_gather x1 -> x0, blocking collectives: 15.8 us -> none  [shards(): lax.all_gather(jnp.concatenate([ctx_keys, ctx_values], axis=-1), 'sp', ax...]
    ppermute x0 -> x3, waiting for transfers between devices: none -> 11.4 us  [collect(): pieces.append(lax.ppermute(pieces[-1], axis, right))]
    ppermute x0 -> x3, starting transfers between devices: none -> 4.13 us  [collect(): pieces.append(lax.ppermute(pieces[-1], axis, right))]
  transfers between devices with their start and end apart: 4 -> 7, of which waited for: 0 -> 2; matrix products, arithmetic and copies ran while one was open for 45% -> 44% of each run, Pallas kernels for 0% -> 0%
where the time goes in v1:
time: 225 us; the launch traced here: 224 us
  matrix products  71.2 us (32%)
  blocking collectives  50.3 us (22%)
  other arithmetic  37 us (16%)
  local copies, waits for them, and re-layouts  19.4 us (9%)
  between operations  13.7 us (6%)
  waiting for transfers between devices  11.4 us (5%)
  loops' own time  10.7 us (5%)
  starting transfers between devices  10.2 us (5%)
    psum x1, blocking collectives, shards(): lax.psum((jnp.dot(active, w_shift, preferred_element_type=jnp.float32), j...  21.3 us
    reduce_sum x4, other arithmetic, attend(): far_exp.sum(-1, keepdims=True)  21 us
    dot_general x4, matrix products, attend(): jnp.einsum('qgrd,kgd->grqk', q_rows, far_keys, preferred_element_type=jnp...  18.3 us
    all_gather x1, blocking collectives, shards(): lax.all_gather(gate_part, 'tp', axis=1, tiled=True)  12.7 us
    ppermute x3, waiting for transfers between devices, collect(): pieces.append(lax.ppermute(pieces[-1], axis, right))  11.4 us
    another operation x1, loops' own time, shards(): lax.map(attend, jnp.arange(samples * blocks, dtype=jnp.int32))  10.7 us
    dot_general x4, matrix products, attend(): jnp.einsum('grqk,kgd->qgrd', (far_exp / normaliser).astype(jnp.bfloat16),...  8.49 us
    all_gather x1, blocking collectives, shards(): lax.all_gather(shift_part, 'tp', axis=1, tiled=True)  8.18 us
  transfers between devices with their start and end apart: 7, of which 2 were waited for; matrix products, arithmetic and copies ran while one was open for 44% of the time, Pallas kernels for 0%

profile of v1, /device:TPU:0, one launch (start us, length us, event | category | flops | bytes accessed | tf_op | source)
XLA Modules:
  0.0 223.9 jit_solution(14824014929606318940)
XLA Ops:
  6.6 0.8 broadcast_in_dim.31
  7.3 1.2 fusion.72
  8.6 1.2 fusion.74
  9.8 1.2 fusion.76
  11.1 21.3 %all-reduce = (f32[3,512]{1,0:T(4,128)S(1)}, f32[3,512]{1,0:T(4,128)S(1)}, f32[3,512]{1,0:T(4,128)}) all-reduce(f32[3,512]{1,0:T(4,128)S(1)} %fusion.72, f32[3,512]{1,0:T(4,128)S(1)} %fusion.74, f32[3,512]{1,0:T(4,128)S(1)} %fusion.76), channel_id=1, replica_groups=mesh['sp'=4,'tp'=4,'dp'=2] {'sp'}, use_global_device_ids=true, to_apply=%region_3.4 | all-reduce | flops 4608 | bytes 36864 | tf_op jit(solution)/shard_map/psum | solution.py:100
  32.3 8.2 %all_gather.14 = f32[3,2048]{1,0:T(4,128)S(1)} all-gather(f32[3,512]{1,0:T(4,128)S(1)} %get-tuple-element.196), channel_id=1, replica_groups=mesh['sp'=4,'tp'=4,'dp'=2] {'tp'}, dimensions={1}, use_global_device_ids=true | all-gather | bytes 30720 | tf_op jit(solution)/shard_map/all_gather | solution.py:109
  40.5 8.2 %all_gather.13 = f32[3,2048]{1,0:T(4,128)S(1)} all-gather(f32[3,512]{1,0:T(4,128)S(1)} %get-tuple-element.197), channel_id=1, replica_groups=mesh['sp'=4,'tp'=4,'dp'=2] {'tp'}, dimensions={1}, use_global_device_ids=true | all-gather | bytes 30720 | tf_op jit(solution)/shard_map/all_gather | solution.py:110
  48.7 5.1 %fusion.26 = f32[2,1024]{1,0:T(2,128)S(1)} fusion(bf16[2,1024,2048]{2,1,0:T(8,128)(2,1)} %param.16), kind=kLoop, calls=%fused_computation.45 | loop fusion | flops 12580864 | bytes 8396800 | tf_op jit(solution)/shard_map/reduce_sum | solution.py:50
  53.8 0.5 multiply_cosine_fusion
  54.4 6.0 %convolution_bitcast_fusion = f32[2,1024,1,64]{1,3,0,2:T(8,128)S(1)} fusion(bf16[2,1024,2048]{2,1,0:T(8,128)(2,1)} %param.16, f32[2,2048]{1,0:T(2,128)S(1)} %slice.76, f32[2,2048]{1,0:T(2,128)S(1)} %slice_add_fusion, f32[2048]{0:T(1024)S(1)} %copy-done.7, f32[2,1024]{1,0:T(2,128)S(1)} %add_rsqrt_fusion, bf16[2048,64]{0,1:T(8,128)(2,1)S(1)} %copy-done.6), kind=kOutput, calls=%fused_computation.60 | convolution fusion | flops 562036736 | bytes 9224192 | tf_op jit(solution)/shard_map/snd,dc->snc/dot_general | solution.py:129
  60.6 7.1 %fusion.40 = bf16[2,1024,128]{1,2,0:T(8,128)(2,1)S(1)} fusion(bf16[2,1024,128]{1,2,0:T(8,128)(2,1)S(1)} %fusion.59, bf16[2,1024,2048]{2,1,0:T(8,128)(2,1)} %param.16, f32[2,2048]{1,0:T(2,128)S(1)} %slice.76, f32[2,2048]{1,0:T(2,128)S(1)} %slice_add_fusion, f32[2048]{0:T(1024)S(1)} %copy-done.7, f32[2,1024]{1,0:T(2,128)S(1)} %add_rsqrt_fusion, ...), kind=kOutput, calls=%fused_computation.62 | convolution fusion | flops 562167808 | bytes 8962048 | tf_op jit(solution)/shard_map/snd,dc->snc/dot_general | solution.py:134
  67.7 1.3 collective-permute-start
  69.0 1.3 collective-permute-start.1
  70.8 1.0 convolution_convert_fusion.1
  71.9 1.0 convolution_convert_fusion.2
  72.9 2.9 %collective-permute-start.2 = (bf16[2,256,128]{1,2,0:T(8,128)(2,1)S(1)}, bf16[2,256,128]{1,2,0:T(8,128)(2,1)S(1)}, u32[]{:S(2)}, u32[]{:S(2)}) collective-permute-start(bf16[2,256,128]{1,2,0:T(8,128)(2,1)S(1)} %get-tuple-element.212), channel_id=1, source_target_pairs={{0,8},{8,16},{16,24},{24,0},{1,9},{9,17},{17,25},{25,1},{2,10},{10... | collective-permute-start | bytes 393224 | tf_op jit(solution)/shard_map/ppermute | solution.py:25
  75.8 6.3 %fusion.43 = f32[2,1024,256]{1,2,0:T(8,128)S(1)} fusion(bf16[2048,256]{1,0:T(8,128)(2,1)S(1)} %copy-done, bf16[2,1024,2048]{2,1,0:T(8,128)(2,1)} %param.16, f32[2,2048]{1,0:T(2,128)S(1)} %slice.76, f32[2,2048]{1,0:T(2,128)S(1)} %slice_add_fusion, f32[2048]{0:T(1024)S(1)} %copy-done.7, f32[2,1024]{1,0:T(2,128)S(1)} %add_rsqrt_fusion), kind=kOutput, calls=%fused_computation.66 | convolution fusion | flops 2172649472 | bytes 11583488 | tf_op jit(solution)/shard_map/snd,dc->snc/dot_general | solution.py:123
  82.6 1.3 collective-permute-start.3
  83.9 5.5 %collective-permute-done.3 = bf16[2,256,128]{1,2,0:T(8,128)(2,1)S(1)} collective-permute-done((bf16[2,256,128]{1,2,0:T(8,128)(2,1)S(1)}, bf16[2,256,128]{1,2,0:T(8,128)(2,1)S(1)}, u32[]{:S(2)}, u32[]{:S(2)}) %collective-permute-start.3) | collective-permute-done | bytes 131104 | tf_op jit(solution)/shard_map/ppermute | solution.py:25
  89.5 0.9 pad_maximum_fusion.1
  90.4 5.8 %collective-permute-done.4 = bf16[2,256,128]{1,2,0:T(8,128)(2,1)S(1)} collective-permute-done((bf16[2,256,128]{1,2,0:T(8,128)(2,1)S(1)}, bf16[2,256,128]{1,2,0:T(8,128)(2,1)S(1)}, u32[]{:S(2)}, u32[]{:S(2)}) %collective-permute-start.4) | collective-permute-done | bytes 131104 | tf_op jit(solution)/shard_map/ppermute | solution.py:25
  96.3 0.6 gather_fusion
  97.2 0.6 iota.45
  97.7 93.7 %while.13 = (s32[]{:T(128)}, bf16[4,512,256]{2,1,0:T(8,128)(2,1)}, s32[4]{0:T(128)}, bf16[2,1280,128]{1,2,0:T(8,128)(2,1)}, s32[]{:T(128)}, /*index=5*/bf16[2,10...) while((s32[]{:T(128)}, bf16[4,512,256]{2,1,0:T(8,128)(2,1)}, ...), condition=%wide.region_10.11_spmd, body=%wide.region_5.10_spmd.sunk | while | flops 985405696 | bytes 75716256 | solution.py:212
  97.7 1.3 dynamic_slice.51
  101.8 4.6 %bitcast_reduce_fusion.2 = (f32[4,512]{1,0:T(4,128)S(1)}, f32[1024,512,4]{1,0,2:T(8,128)}) fusion(f32[4]{0:T(128)S(1)} %bitcast.209, bf16[2,1024,4,64]{1,3,2,0:T(8,128)(2,1)S(1)} %get-tuple-element.323, s32[]{:T(128)S(6)} %select_n.154, s32[]{:T(128)S(6)} %select_n.157, bf16[1024,128]{0,1:T(8,128)(2,1)S(1)} %bitcast.196), kind=kOutput, calls=%fused_computation.2.clone.1 | convolution fusion | flops 274724864 | bytes 8790536 | tf_op jit(solution)/shard_map/while/body/eval_jaxpr/qgrd,kgd->grqk/dot_general | solution.py:183
  106.9 1.1 dynamic-slice_bitcast_fusion.2
  108.0 1.3 fusion.95
  109.4 5.2 %fusion.97 = f32[4,512]{1,0:T(4,128)S(1)} fusion(f32[1024,512,4]{1,0,2:T(8,128)} %get-tuple-element.280, f32[4,512]{1,0:T(4,128)S(1)} %maximum_maximum_fusion.2, f32[4]{0:T(128)S(1)} %bitcast.210), kind=kLoop, calls=%fused_computation.6.clone.1 | loop fusion | flops 8386560 | bytes 8405008 | tf_op jit(solution)/shard_map/while/body/eval_jaxpr/reduce_sum | solution.py:195
  114.7 1.4 fusion.96
  116.2 2.1 fusion.98
  118.3 2.0 fusion.99
  120.5 0.7 constant_dynamic-update-slice_fusion.2
  121.2 1.3 dynamic_slice.51
  125.2 4.6 %bitcast_reduce_fusion.2 = (f32[4,512]{1,0:T(4,128)S(1)}, f32[1024,512,4]{1,0,2:T(8,128)}) fusion(f32[4]{0:T(128)S(1)} %bitcast.209, bf16[2,1024,4,64]{1,3,2,0:T(8,128)(2,1)S(1)} %get-tuple-element.323, s32[]{:T(128)S(6)} %select_n.154, s32[]{:T(128)S(6)} %select_n.157, bf16[1024,128]{0,1:T(8,128)(2,1)S(1)} %bitcast.196), kind=kOutput, calls=%fused_computation.2.clone.1 | convolution fusion | flops 274724864 | bytes 8790536 | tf_op jit(solution)/shard_map/while/body/eval_jaxpr/qgrd,kgd->grqk/dot_general | solution.py:183
  130.4 1.1 dynamic-slice_bitcast_fusion.2
  131.4 1.3 fusion.95
  132.8 5.2 %fusion.97 = f32[4,512]{1,0:T(4,128)S(1)} fusion(f32[1024,512,4]{1,0,2:T(8,128)} %get-tuple-element.280, f32[4,512]{1,0:T(4,128)S(1)} %maximum_maximum_fusion.2, f32[4]{0:T(128)S(1)} %bitcast.210), kind=kLoop, calls=%fused_computation.6.clone.1 | loop fusion | flops 8386560 | bytes 8405008 | tf_op jit(solution)/shard_map/while/body/eval_jaxpr/reduce_sum | solution.py:195
  138.1 1.4 fusion.96
  139.6 2.1 fusion.98
  141.7 2.0 fusion.99
  143.9 0.7 constant_dynamic-update-slice_fusion.2
  144.6 1.3 dynamic_slice.51
  148.6 4.6 %bitcast_reduce_fusion.2 = (f32[4,512]{1,0:T(4,128)S(1)}, f32[1024,512,4]{1,0,2:T(8,128)}) fusion(f32[4]{0:T(128)S(1)} %bitcast.209, bf16[2,1024,4,64]{1,3,2,0:T(8,128)(2,1)S(1)} %get-tuple-element.323, s32[]{:T(128)S(6)} %select_n.154, s32[]{:T(128)S(6)} %select_n.157, bf16[1024,128]{0,1:T(8,128)(2,1)S(1)} %bitcast.196), kind=kOutput, calls=%fused_computation.2.clone.1 | convolution fusion | flops 274724864 | bytes 8790536 | tf_op jit(solution)/shard_map/while/body/eval_jaxpr/qgrd,kgd->grqk/dot_general | solution.py:183
  153.8 1.1 dynamic-slice_bitcast_fusion.2
  154.9 1.3 fusion.95
  156.3 5.2 %fusion.97 = f32[4,512]{1,0:T(4,128)S(1)} fusion(f32[1024,512,4]{1,0,2:T(8,128)} %get-tuple-element.280, f32[4,512]{1,0:T(4,128)S(1)} %maximum_maximum_fusion.2, f32[4]{0:T(128)S(1)} %bitcast.210), kind=kLoop, calls=%fused_computation.6.clone.1 | loop fusion | flops 8386560 | bytes 8405008 | tf_op jit(solution)/shard_map/while/body/eval_jaxpr/reduce_sum | solution.py:195
  161.5 1.4 fusion.96
  163.0 2.1 fusion.98
  165.1 2.0 fusion.99
  167.3 0.7 constant_dynamic-update-slice_fusion.2
  168.0 1.3 dynamic_slice.51
  172.1 4.6 %bitcast_reduce_fusion.2 = (f32[4,512]{1,0:T(4,128)S(1)}, f32[1024,512,4]{1,0,2:T(8,128)}) fusion(f32[4]{0:T(128)S(1)} %bitcast.209, bf16[2,1024,4,64]{1,3,2,0:T(8,128)(2,1)S(1)} %get-tuple-element.323, s32[]{:T(128)S(6)} %select_n.154, s32[]{:T(128)S(6)} %select_n.157, bf16[1024,128]{0,1:T(8,128)(2,1)S(1)} %bitcast.196), kind=kOutput, calls=%fused_computation.2.clone.1 | convolution fusion | flops 274724864 | bytes 8790536 | tf_op jit(solution)/shard_map/while/body/eval_jaxpr/qgrd,kgd->grqk/dot_general | solution.py:183
  177.2 1.1 dynamic-slice_bitcast_fusion.2
  178.3 1.3 fusion.95
  179.7 5.2 %fusion.97 = f32[4,512]{1,0:T(4,128)S(1)} fusion(f32[1024,512,4]{1,0,2:T(8,128)} %get-tuple-element.280, f32[4,512]{1,0:T(4,128)S(1)} %maximum_maximum_fusion.2, f32[4]{0:T(128)S(1)} %bitcast.210), kind=kLoop, calls=%fused_computation.6.clone.1 | loop fusion | flops 8386560 | bytes 8405008 | tf_op jit(solution)/shard_map/while/body/eval_jaxpr/reduce_sum | solution.py:195
  184.9 1.4 fusion.96
  186.4 2.1 fusion.98
  188.5 2.0 fusion.99
  190.7 0.7 constant_dynamic-update-slice_fusion.2
  191.4 3.3 %copy.31 = bf16[2,1024,256]{2,0,1:T(2,128)(2,1)} copy(bf16[2,1024,256]{2,1,0:T(8,128)(2,1)} %bitcast.203) | data formatting | bytes 2097152 | tf_op jit(solution)/shard_map/reshape | solution.py:212
  194.7 3.5 %all-to-all-start = ((bf16[2,1024,256]{2,0,1:T(2,128)(2,1)}), bf16[2,1024,256]{2,0,1:T(2,128)(2,1)S(1)}, u32[]{:S(2)}, u32[]{:S(2)}) async-start(bf16[2,1024,256]{2,0,1:T(2,128)(2,1)} %copy.31), calls=%async_computation | async-start | bytes 2097152 | tf_op jit(solution)/shard_map/all_to_all | solution.py:215
  198.2 12.7 %all_gather.12 = f32[3,2048]{1,0:T(4,128)S(1)} all-gather(f32[3,512]{1,0:T(4,128)S(1)} %copy-done.4), channel_id=1, replica_groups=mesh['sp'=4,'tp'=4,'dp'=2] {'tp'}, dimensions={1}, use_global_device_ids=true | all-gather | bytes 30720 | tf_op jit(solution)/shard_map/all_gather | solution.py:111
  211.2 5.8 %multiply_convert_fusion = bf16[2,256,2048]{2,1,0:T(8,128)(2,1)} fusion(bf16[2,256,1024]{2,1,0:T(8,128)(2,1)S(1)} %bitcast.204, bf16[1024,2048]{1,0:T(8,128)(2,1)} %all-gather.2.cloned.1.call-done, f32[2,2048]{1,0:T(2,128)S(1)} %slice.74), kind=kOutput, calls=%fused_computation.59 | convolution fusion | flops 2149580800 | bytes 7356416 | tf_op jit(solution)/shard_map/snc,cd->snd/dot_general | solution.py:216
  (105 shorter events, 5.9 us)
Async XLA Ops:
  6.5 69.3 %copy-start = (bf16[2048,256]{1,0:T(8,128)(2,1)S(1)}, bf16[2048,256]{1,0:T(8,128)(2,1)}, u32[]{:S(2)}) copy-start(bf16[2048,256]{1,0:T(8,128)(2,1)} %param.24) | copy-start | bytes 3145732
  6.5 47.8 %copy-start.7 = (f32[2048]{0:T(1024)S(1)}, f32[2048]{0:T(1024)}, u32[]{:S(2)}) copy-start(f32[2048]{0:T(1024)} %param.20) | copy-start | bytes 24580
  6.5 47.9 %copy-start.6 = (bf16[2048,64]{0,1:T(8,128)(2,1)S(1)}, bf16[2048,64]{0,1:T(8,128)(2,1)}, u32[]{:S(2)}) copy-start(bf16[2048,64]{0,1:T(8,128)(2,1)} %param.25) | copy-start | bytes 786436
  6.5 204.7 %all-gather.2.cloned.1.call-start = ((), (), s32[]{:S(2)}) async-start(), calls=%async_computation.1 | async-start | bytes 5242880 | tf_op jit(solution)/shard_map/all_gather | solution.py:219
  54.4 6.1 %copy-start.5 = (bf16[2048,64]{0,1:T(8,128)(2,1)S(1)}, bf16[2048,64]{0,1:T(8,128)(2,1)}, u32[]{:S(2)}) copy-start(bf16[2048,64]{0,1:T(8,128)(2,1)} %param.26) | copy-start | bytes 786436
  60.5 9.8 %copy-start.1 = (bf16[2,256,2048]{2,1,0:T(8,128)(2,1)S(1)}, bf16[2,256,2048]{2,1,0:T(8,128)(2,1)}, u32[]{:S(2)}) copy-start(bf16[2,256,2048]{2,1,0:T(8,128)(2,1)} %param.17) | copy-start | bytes 6291460
  67.7 21.8 %collective-permute-start = (bf16[2,128,128]{1,2,0:T(8,128)(2,1)S(1)}, bf16[2,128,128]{1,2,0:T(8,128)(2,1)S(1)}, u32[]{:S(2)}, u32[]{:S(2)}) collective-permute-start(bf16[2,128,128]{1,2,0:T(8,128)(2,1)S(1)} %get-tuple-element.209), channel_id=1, source_target_pairs={{0,8},{8,16},{16,24},{1,9},{9,17},{17,25},{2,10},{10,18},{18,26},{... | collective-permute-start | bytes 196616 | tf_op jit(solution)/shard_map/ppermute | solution.py:39
  69.0 20.5 %collective-permute-start.1 = (bf16[2,128,128]{1,2,0:T(8,128)(2,1)S(1)}, bf16[2,128,128]{1,2,0:T(8,128)(2,1)S(1)}, u32[]{:S(2)}, u32[]{:S(2)}) collective-permute-start(bf16[2,128,128]{1,2,0:T(8,128)(2,1)S(1)} %get-tuple-element.210), channel_id=1, source_target_pairs={{8,0},{16,8},{24,16},{9,1},{17,9},{25,17},{10,2},{18,10},{26,18},{... | collective-permute-start | bytes 196616 | tf_op jit(solution)/shard_map/ppermute | solution.py:41
  72.9 9.7 %collective-permute-start.2 = (bf16[2,256,128]{1,2,0:T(8,128)(2,1)S(1)}, bf16[2,256,128]{1,2,0:T(8,128)(2,1)S(1)}, u32[]{:S(2)}, u32[]{:S(2)}) collective-permute-start(bf16[2,256,128]{1,2,0:T(8,128)(2,1)S(1)} %get-tuple-element.212), channel_id=1, source_target_pairs={{0,8},{8,16},{16,24},{24,0},{1,9},{9,17},{17,25},{25,1},{2,10},{10... | collective-permute-start | bytes 393224 | tf_op jit(solution)/shard_map/ppermute | solution.py:25
  82.1 15.6 %copy-start.2 = (f32[4]{0:T(128)S(1)}, f32[4]{0:T(128)}, u32[]{:S(2)}) copy-start(f32[4]{0:T(128)} %param.29) | copy-start | bytes 52
  82.2 15.6 %copy-start.3 = (f32[4]{0:T(128)S(1)}, f32[4]{0:T(128)}, u32[]{:S(2)}) copy-start(f32[4]{0:T(128)} %param.28) | copy-start | bytes 52
  82.6 6.8 %collective-permute-start.3 = (bf16[2,256,128]{1,2,0:T(8,128)(2,1)S(1)}, bf16[2,256,128]{1,2,0:T(8,128)(2,1)S(1)}, u32[]{:S(2)}, u32[]{:S(2)}) collective-permute-start(bf16[2,256,128]{1,2,0:T(8,128)(2,1)S(1)} %collective-permute-done.2), channel_id=1, source_target_pairs={{0,8},{8,16},{16,24},{24,0},{1,9},{9,17},{17,25},{25,1},{2,10},{10... | collective-permute-start | bytes 393224 | tf_op jit(solution)/shard_map/ppermute | solution.py:25
  89.5 6.8 %collective-permute-start.4 = (bf16[2,256,128]{1,2,0:T(8,128)(2,1)S(1)}, bf16[2,256,128]{1,2,0:T(8,128)(2,1)S(1)}, u32[]{:S(2)}, u32[]{:S(2)}) collective-permute-start(bf16[2,256,128]{1,2,0:T(8,128)(2,1)S(1)} %collective-permute-done.3), channel_id=1, source_target_pairs={{0,8},{8,16},{16,24},{24,0},{1,9},{9,17},{17,25},{25,1},{2,10},{10... | collective-permute-start | bytes 393224 | tf_op jit(solution)/shard_map/ppermute | solution.py:25
  97.7 100.5 %copy-start.4 = (f32[3,512]{1,0:T(4,128)S(1)}, f32[3,512]{1,0:T(4,128)}, u32[]{:S(2)}) copy-start(f32[3,512]{1,0:T(4,128)} %get-tuple-element.198) | copy-start | bytes 18436
  109.4 6.7 %slice-start = ((s8[8388608]{0:T(1024)(128)(4,1)}), s8[4194304]{0:T(1024)(128)(4,1)S(1)}, s32[]{:S(2)}) async-start(s8[8388608]{0:T(1024)(128)(4,1)} %bitcast.194), calls=%async_computation.2 | async-start | bytes 8388608 | tf_op jit(solution)/shard_map/while
  109.4 6.7 %slice-start.1 = ((s8[8388608]{0:T(1024)(128)(4,1)}), s8[4194304]{0:T(1024)(128)(4,1)S(1)}, s32[]{:S(2)}) async-start(s8[8388608]{0:T(1024)(128)(4,1)} %bitcast.194), calls=%async_computation.3 | async-start | bytes 8388608 | tf_op jit(solution)/shard_map/while
  132.8 6.7 %slice-start = ((s8[8388608]{0:T(1024)(128)(4,1)}), s8[4194304]{0:T(1024)(128)(4,1)S(1)}, s32[]{:S(2)}) async-start(s8[8388608]{0:T(1024)(128)(4,1)} %bitcast.194), calls=%async_computation.2 | async-start | bytes 8388608 | tf_op jit(solution)/shard_map/while
  132.8 6.7 %slice-start.1 = ((s8[8388608]{0:T(1024)(128)(4,1)}), s8[4194304]{0:T(1024)(128)(4,1)S(1)}, s32[]{:S(2)}) async-start(s8[8388608]{0:T(1024)(128)(4,1)} %bitcast.194), calls=%async_computation.3 | async-start | bytes 8388608 | tf_op jit(solution)/shard_map/while
  156.3 6.7 %slice-start = ((s8[8388608]{0:T(1024)(128)(4,1)}), s8[4194304]{0:T(1024)(128)(4,1)S(1)}, s32[]{:S(2)}) async-start(s8[8388608]{0:T(1024)(128)(4,1)} %bitcast.194), calls=%async_computation.2 | async-start | bytes 8388608 | tf_op jit(solution)/shard_map/while
  156.3 6.7 %slice-start.1 = ((s8[8388608]{0:T(1024)(128)(4,1)}), s8[4194304]{0:T(1024)(128)(4,1)S(1)}, s32[]{:S(2)}) async-start(s8[8388608]{0:T(1024)(128)(4,1)} %bitcast.194), calls=%async_computation.3 | async-start | bytes 8388608 | tf_op jit(solution)/shard_map/while
  179.7 6.7 %slice-start = ((s8[8388608]{0:T(1024)(128)(4,1)}), s8[4194304]{0:T(1024)(128)(4,1)S(1)}, s32[]{:S(2)}) async-start(s8[8388608]{0:T(1024)(128)(4,1)} %bitcast.194), calls=%async_computation.2 | async-start | bytes 8388608 | tf_op jit(solution)/shard_map/while
  179.7 6.7 %slice-start.1 = ((s8[8388608]{0:T(1024)(128)(4,1)}), s8[4194304]{0:T(1024)(128)(4,1)S(1)}, s32[]{:S(2)}) async-start(s8[8388608]{0:T(1024)(128)(4,1)} %bitcast.194), calls=%async_computation.3 | async-start | bytes 8388608 | tf_op jit(solution)/shard_map/while
  194.7 16.2 %all-to-all-start = ((bf16[2,1024,256]{2,0,1:T(2,128)(2,1)}), bf16[2,1024,256]{2,0,1:T(2,128)(2,1)S(1)}, u32[]{:S(2)}, u32[]{:S(2)}) async-start(bf16[2,1024,256]{2,0,1:T(2,128)(2,1)} %copy.31), calls=%async_computation | async-start | bytes 2097152 | tf_op jit(solution)/shard_map/all_to_all | solution.py:215
Sparse Core Ops, SparseCore 0:
  76.0 50.4 all-gather.1
